TPU v7x, 32 devices: a whole 2x2x4 slice. The times are simulated.
32 devices in a mesh: sp: 4 (over y, x), tp: 8 (over z, core).
Axes of the slice: x: 2, y: 2, z: 4, core: 2. Of those that a mesh axis runs over, the one named last changes fastest.
Arguments:
- cotangent: bfloat16 [1024, 2048], P('sp', 'tp'), may hold values from -6 to 6
- block_input: bfloat16 [1024, 2048], P('sp', 'tp'), may hold values from -6 to 6
- routes: int32 [1024, 2], P('sp'), may hold values from 0 to 3, all different within a row; in each aligned block of 256 rows (0 to 255, 256 to 511, ...) at most 160 rows name the same one
- route_weights: float32 [1024, 2], P('sp'), may hold values from 0.1 to 0.9
- gate_weight: bfloat16 [4, 2048, 7168], P('sp', None, 'tp'), may hold values from -0.125 to 0.125
- up_weight: bfloat16 [4, 2048, 7168], P('sp', None, 'tp'), may hold values from -0.125 to 0.125
- down_weight: bfloat16 [4, 7168, 2048], P('sp', 'tp'), may hold values from -0.0625 to 0.0625
- out_weight: bfloat16 [1024, 2048], P('tp'), may hold values from -0.1875 to 0.1875
- conv_out: bfloat16 [1024, 1024], P('tp', 'sp'), may hold values from -6 to 6
- gate_pre: bfloat16 [1024, 1024], P('tp', 'sp'), may hold values from -6 to 6
- prior_states: bfloat16 [1024, 1024], P('tp', 'sp'), may hold values from -6 to 6
- recur_weight: bfloat16 [16, 64, 64], replicated, may hold values from -0.75 to 0.75
- input_gate_matrix: bfloat16 [16, 64, 64], replicated, may hold values from -0.75 to 0.75
- decay_param: float32 [1024], replicated, may hold values from 4 to 16
- decay_jump: float32 [1024, 1024], P('tp', 'sp'), may hold values from -1 to 0, as said below
Outputs:
- gate_weight_grad: bfloat16 [4, 2048, 7168], P('sp', None, 'tp')
- up_weight_grad: bfloat16 [4, 2048, 7168], P('sp', None, 'tp')
- down_weight_grad: bfloat16 [4, 7168, 2048], P('sp', 'tp')
- out_weight_grad: float32 [1024, 2048], P('tp', 'sp')
- conv_grad: bfloat16 [1024, 1024], P('tp', 'sp')
- valve_logit_derivative: bfloat16 [1024, 1024], P('tp', 'sp')
Inputs may be any that keep to these rules, and one draw needn't show every extreme that they name: In each aligned block of 256 rows (the rows of one index of sp) no expert is named by more than 160 routes, a bound that some block reaches; a row names 2 different experts. `decay_jump`: every entry is at most -1 / 20480.
All inputs are finite; a program needn't handle non-finite values.
Results may differ from a plain program's by a relative error of at most 0.018.
Values may be sent and summed in bfloat16 or wider, within the bound.
A program may use at most 128 MiB of HBM per device.

v0:
```python
import jax
import jax.numpy as jnp
from jax import lax
from jax.sharding import PartitionSpec as P

HEAD_DIM = 64
TOP_K = 2
RATE_SCALE = 8.0


def prefix(value, axis, join, neutral):
    count, mine = (lax.axis_size(axis), lax.axis_index(axis))
    pieces = jax.tree.map(lambda part: lax.all_gather(part, axis), value)
    pieces = jax.tree.map(lambda part: part[::-1], pieces)
    mine = count - 1 - mine
    so_far = jax.tree.map(
        lambda part, zero: jnp.full_like(part, 0) + jnp.asarray(zero, part.dtype), value, neutral
    )

    def turn(position, so_far):
        longer = join(so_far, jax.tree.map(lambda part: part[position], pieces))
        return jax.tree.map(lambda new, old: jnp.where(position < mine, new, old), longer, so_far)

    return lax.fori_loop(0, count - 1, turn, so_far)


def link_pairs(left_pair, right_pair):
    return (left_pair[0] * right_pair[0], right_pair[0] * left_pair[1] + right_pair[1])


def later_first(earlier_pair, later_pair):
    return (earlier_pair[0] * later_pair[0], later_pair[1] + later_pair[0] * earlier_pair[1])


def routing_tables(routes, experts, capacity):
    flat_routes = routes.reshape(-1)
    onehot = (flat_routes[:, None] == jnp.arange(experts, dtype=jnp.int32)[None, :]).astype(
        jnp.int32
    )
    slot_rank = jnp.sum((jnp.cumsum(onehot, axis=0) - onehot) * onehot, axis=1)
    target = (flat_routes * capacity + slot_rank).reshape(routes.shape[0], routes.shape[1])
    slot_ids = jnp.arange(experts * capacity, dtype=jnp.int32)
    return jnp.transpose(target)[:, None, :] == slot_ids[None, :, None]


def spread(placing, route_hits, rows_in, cot_in, route_weights):
    sent_rows = jnp.dot(placing, rows_in, preferred_element_type=jnp.float32).astype(jnp.bfloat16)
    scaled = (
        jnp.transpose(route_weights)[:, :, None] * cot_in.astype(jnp.float32)[None, :, :]
    ).astype(jnp.bfloat16)
    sent_cot = jnp.einsum(
        "kst,ktd->sd", route_hits, scaled, preferred_element_type=jnp.float32
    ).astype(jnp.bfloat16)
    return (sent_rows, sent_cot)


def expert_work(slot_rows, slot_cot, w_gate, w_up, w_down):
    minor = (((1,), (1,)), ((), ()))
    gate_act = jnp.dot(slot_rows, w_gate, preferred_element_type=jnp.float32)
    up_act = jnp.dot(slot_rows, w_up, preferred_element_type=jnp.float32)
    sigma_gate = jax.nn.sigmoid(gate_act)
    silu_val = gate_act * sigma_gate
    hidden = (silu_val * up_act).astype(jnp.bfloat16)
    d_hidden = lax.dot_general(slot_cot, w_down, minor, preferred_element_type=jnp.float32)
    d_gate = (d_hidden * up_act * sigma_gate * (1.0 + gate_act * (1.0 - sigma_gate))).astype(
        jnp.bfloat16
    )
    d_up = (d_hidden * silu_val).astype(jnp.bfloat16)
    width_part = lax.dot_general(d_gate, w_gate, minor, preferred_element_type=jnp.float32)
    width_part = width_part + lax.dot_general(d_up, w_up, minor, preferred_element_type=jnp.float32)
    return (hidden, d_gate, d_up, width_part)


def weight_grads(slot_rows, slot_cot, hidden, d_gate, d_up):
    major = (((0,), (0,)), ((), ()))
    gate_grad = lax.dot_general(
        slot_rows, d_gate, major, preferred_element_type=jnp.float32
    ).astype(jnp.bfloat16)
    up_grad = lax.dot_general(slot_rows, d_up, major, preferred_element_type=jnp.float32).astype(
        jnp.bfloat16
    )
    down_grad = lax.dot_general(hidden, slot_cot, major, preferred_element_type=jnp.float32).astype(
        jnp.bfloat16
    )
    return (gate_grad[None], up_grad[None], down_grad[None])


def local(
    cotangent,
    block_input,
    routes,
    route_weights,
    gate_weight,
    up_weight,
    down_weight,
    out_weight,
    conv_out,
    gate_pre,
    prior_states,
    recur_weight,
    input_gate_matrix,
    decay_param,
    decay_jump,
):
    experts = lax.axis_size("sp")
    tok_rows = cotangent.shape[0]
    capacity = 5 * tok_rows * TOP_K // (4 * experts)
    route_hits = routing_tables(routes, experts, capacity)
    placing = jnp.sum(route_hits.astype(jnp.int32), axis=0).astype(jnp.bfloat16)
    hit_table = route_hits.astype(jnp.bfloat16)
    sent_rows, sent_cot = spread(placing, hit_table, block_input, cotangent, route_weights)
    part_rows, portion_adjoint = (
        lax.all_to_all(
            sent_rows.reshape(experts, capacity, -1), "sp", split_axis=0, concat_axis=0, tiled=True
        ),
        lax.all_to_all(
            sent_cot.reshape(experts, capacity, -1), "sp", split_axis=0, concat_axis=0, tiled=True
        ),
    )
    got_rows, got_cot = (
        lax.all_gather(part_rows, "tp", axis=2, tiled=True),
        lax.all_gather(portion_adjoint, "tp", axis=2, tiled=True),
    )
    full_width = got_rows.shape[2]
    slot_rows = got_rows.reshape(-1, full_width)
    slot_cot = got_cot.reshape(-1, full_width)
    hidden, d_gate, d_up, width_part = expert_work(
        slot_rows, slot_cot, gate_weight[0], up_weight[0], down_weight[0]
    )
    gate_grad, up_grad, down_grad = weight_grads(slot_rows, slot_cot, hidden, d_gate, d_up)
    summed = lax.psum_scatter(
        width_part.reshape(experts, capacity, full_width).astype(jnp.bfloat16),
        "tp",
        scatter_dimension=2,
        tiled=True,
    )
    handed_result = lax.all_to_all(summed, "sp", split_axis=0, concat_axis=0, tiled=True).reshape(
        experts * capacity, -1
    )
    moe_grad = lax.dot_general(
        placing, handed_result, (((0,), (0,)), ((), ())), preferred_element_type=jnp.float32
    )
    block_grad = (cotangent.astype(jnp.float32) + moe_grad).astype(jnp.bfloat16)
    full_grad = lax.all_gather(block_grad, "tp", axis=1, tiled=True)
    channels = conv_out.shape[0]
    length = conv_out.shape[1]
    head_count = channels // HEAD_DIM
    head_start = lax.axis_index("tp") * head_count
    w_recur = lax.dynamic_slice_in_dim(recur_weight, head_start, head_count, 0)
    w_input = lax.dynamic_slice_in_dim(input_gate_matrix, head_start, head_count, 0)
    rate_parameter = lax.dynamic_slice_in_dim(decay_param, head_start * HEAD_DIM, channels, 0)[
        :, None
    ]
    shaped = conv_out.reshape(head_count, HEAD_DIM, length)
    recur_gate = jax.nn.sigmoid(
        jnp.einsum("hij,hit->hjt", w_recur, shaped, preferred_element_type=jnp.float32).reshape(
            channels, length
        )
    )
    input_gate = jax.nn.sigmoid(
        jnp.einsum("hij,hit->hjt", w_input, shaped, preferred_element_type=jnp.float32).reshape(
            channels, length
        )
    )
    softened = jax.nn.softplus(-rate_parameter)
    log_decay = -RATE_SCALE * recur_gate * softened + decay_jump
    decay_val = jnp.exp(log_decay)
    norm_scale = jnp.sqrt(-jnp.expm1(2.0 * log_decay))
    conv_vals = conv_out.astype(jnp.float32)
    prior_vals = prior_states.astype(jnp.float32)
    state = decay_val * prior_vals + norm_scale * input_gate * conv_vals
    gelu_val, gelu_pull = jax.vjp(jax.nn.gelu, gate_pre.astype(jnp.float32))
    mixed = (gelu_val * state).astype(jnp.bfloat16)
    d_mixed = lax.dot_general(
        out_weight, full_grad, (((1,), (1,)), ((), ())), preferred_element_type=jnp.float32
    )
    valve_logit_derivative = gelu_pull(d_mixed * state)[0].astype(jnp.bfloat16)
    d_state = d_mixed * gelu_val
    shifted = jnp.concatenate([decay_val[:, 1:], jnp.ones((channels, 1), jnp.float32)], axis=1)
    flipped = lax.associative_scan(link_pairs, (jnp.flip(shifted, 1), jnp.flip(d_state, 1)), axis=1)
    decay_prod = jnp.flip(flipped[0], 1)
    local_sum = jnp.flip(flipped[1], 1)
    summary = (decay_val[:, 0] * decay_prod[:, 0], decay_val[:, 0] * local_sum[:, 0])
    carried = prefix(
        summary,
        "sp",
        later_first,
        (jnp.ones((channels,), jnp.float32), jnp.zeros((channels,), jnp.float32)),
    )[1]
    state_grad = local_sum + decay_prod * carried[:, None]
    grad_log = (
        state_grad * prior_vals * decay_val
        - state_grad * input_gate * conv_vals * decay_val * decay_val / norm_scale
    )
    grad_recur = (grad_log * -RATE_SCALE * softened * recur_gate * (1.0 - recur_gate)).astype(
        jnp.bfloat16
    )
    grad_input = (state_grad * norm_scale * conv_vals * input_gate * (1.0 - input_gate)).astype(
        jnp.bfloat16
    )
    back_recur = jnp.einsum(
        "hij,hjt->hit",
        w_recur,
        grad_recur.reshape(head_count, HEAD_DIM, length),
        preferred_element_type=jnp.float32,
    ).reshape(channels, length)
    back_input = jnp.einsum(
        "hij,hjt->hit",
        w_input,
        grad_input.reshape(head_count, HEAD_DIM, length),
        preferred_element_type=jnp.float32,
    ).reshape(channels, length)
    conv_grad = (state_grad * norm_scale * input_gate + back_recur + back_input).astype(
        jnp.bfloat16
    )
    projected = lax.psum_scatter(
        lax.dot_general(
            full_grad, mixed, (((0,), (1,)), ((), ())), preferred_element_type=jnp.float32
        ).astype(jnp.bfloat16),
        "sp",
        scatter_dimension=0,
        tiled=True,
    ).astype(jnp.float32)
    out_weight_grad = jnp.transpose(projected)
    return (gate_grad, up_grad, down_grad, out_weight_grad, conv_grad, valve_logit_derivative)


def solution(mesh):
    in_specs = (
        P("sp", "tp"),
        P("sp", "tp"),
        P("sp", None),
        P("sp", None),
        P("sp", None, "tp"),
        P("sp", None, "tp"),
        P("sp", "tp", None),
        P("tp", None),
        P("tp", "sp"),
        P("tp", "sp"),
        P("tp", "sp"),
        P(),
        P(),
        P(),
        P("tp", "sp"),
    )
    out_specs = (
        P("sp", None, "tp"),
        P("sp", None, "tp"),
        P("sp", "tp", None),
        P("tp", "sp"),
        P("tp", "sp"),
        P("tp", "sp"),
    )
    return jax.shard_map(local, mesh=mesh, in_specs=in_specs, out_specs=out_specs, check_vma=False)
```

profile of v0, /device:TPU:0, one launch (start us, length us, event | category | flops | bytes accessed | tf_op | source)
XLA Modules:
  0.0 229.2 jit_solution(16892057116044407689)
XLA Ops:
  7.2 0.9 copy.72
  8.4 1.2 reduce-window.6
  11.3 1.1 convolution_convert_fusion.1
  12.5 11.7 %all_to_all.15 = bf16[4,160,256]{2,1,0:T(8,128)(2,1)} all-to-all(bf16[4,160,256]{2,1,0:T(8,128)(2,1)S(1)} %bitcast.101), channel_id=1, replica_groups=mesh['sp'=4,'tp'=8] {'sp'}, dimensions={0} | all-to-all | bytes 655360 | tf_op jit(solution)/shard_map/all_to_all | solution.py:113
  24.8 9.3 %all_to_all.16 = bf16[4,160,256]{2,1,0:T(8,128)(2,1)} all-to-all(bf16[4,160,256]{2,1,0:T(8,128)(2,1)S(1)} %bitcast.104), channel_id=1, replica_groups=mesh['sp'=4,'tp'=8] {'sp'}, dimensions={0} | all-to-all | bytes 655360 | tf_op jit(solution)/shard_map/all_to_all | solution.py:116
  34.2 24.6 %all-gather.6.cloned.1.call-done = bf16[4,160,2048]{2,1,0:T(8,128)(2,1)} async-done(((bf16[4,160,256]{2,1,0:T(8,128)(2,1)}), bf16[4,160,2048]{2,1,0:T(8,128)(2,1)}) %all-gather.6.cloned.1.call-update) | async-done | bytes 2621456 | tf_op jit(solution)/shard_map/all_gather | solution.py:121
  58.8 7.2 %fusion.3 = f32[640,896]{1,0:T(8,128)} fusion(bf16[640,2048]{1,0:T(8,128)(2,1)} %bitcast.114, bf16[1,2048,896]{2,1,0:T(8,128)(2,1)} %param.21), kind=kOutput, calls=%fused_computation.7 | convolution fusion | flops 2348810240 | bytes 8585216 | tf_op jit(solution)/shard_map/dot_general | solution.py:59
  66.0 4.3 %fusion.7 = f32[640,896]{1,0:T(8,128)} fusion(bf16[640,2048]{1,0:T(8,128)(2,1)S(1)} %bitcast.116, bf16[1,2048,896]{2,1,0:T(8,128)(2,1)S(1)} %copy-done.8), kind=kOutput, calls=%fused_computation.11 | convolution fusion | flops 2348810240 | bytes 8585216 | tf_op jit(solution)/shard_map/dot_general | solution.py:60
  70.4 23.2 %all-gather.8.cloned.1.call-done = bf16[4,160,2048]{2,1,0:T(8,128)(2,1)} async-done(((bf16[4,160,256]{2,1,0:T(8,128)(2,1)}), bf16[4,160,2048]{2,1,0:T(8,128)(2,1)}) %all-gather.8.cloned.1.call-update) | async-done | bytes 2621456 | tf_op jit(solution)/shard_map/all_gather | solution.py:122
  93.6 7.8 %multiply_convert_fusion.1 = (bf16[640,896]{1,0:T(8,128)(2,1)S(1)}, bf16[640,896]{1,0:T(8,128)(2,1)S(1)}) fusion(f32[640,896]{1,0:T(8,128)} %fusion.3, f32[640,896]{1,0:T(8,128)} %fusion.7, bf16[640,2048]{1,0:T(8,128)(2,1)} %bitcast.118, bf16[1,896,2048]{2,1,0:T(8,128)(2,1)} %param.23), kind=kOutput, calls=%fused_computation.20 | convolution fusion | flops 2356264960 | bytes 13172736 | tf_op jit(solution)/shard_map/dot_general | solution.py:64
  101.5 2.9 %fusion.1 = f32[640,2048]{1,0:T(8,128)S(1)} fusion(bf16[640,896]{1,0:T(8,128)(2,1)S(1)} %get-tuple-element.152, bf16[1,2048,896]{2,1,0:T(8,128)(2,1)S(1)} %copy-done.7), kind=kOutput, calls=%fused_computation.5 | convolution fusion | flops 2348810240 | bytes 10059776 | tf_op jit(solution)/shard_map/dot_general | solution.py:69
  104.4 4.2 %add_convert_fusion = bf16[640,2048]{1,0:T(8,128)(2,1)} fusion(f32[640,2048]{1,0:T(8,128)S(1)} %fusion.1, bf16[640,896]{1,0:T(8,128)(2,1)S(1)} %get-tuple-element.151, bf16[1,2048,896]{2,1,0:T(8,128)(2,1)S(1)} %copy-done.9), kind=kOutput, calls=%fused_computation.4 | convolution fusion | flops 2351431680 | bytes 12681216 | tf_op jit(solution)/shard_map/dot_general | solution.py:70
  108.6 0.8 copy-done.4
  109.5 1.0 fusion.23
  110.7 34.2 %reduce-scatter.3.cloned.1.call-done = bf16[4,160,256]{2,1,0:T(8,128)(2,1)} async-done(((bf16[4,160,2048]{2,1,0:T(8,128)(2,1)}), bf16[4,160,256]{2,1,0:T(8,128)(2,1)}) %reduce-scatter.3.cloned.1.call-update) | async-done | bytes 327696 | tf_op jit(solution)/shard_map/reduce_scatter | solution.py:131
  144.9 3.7 %all-to-all-start.2 = ((bf16[4,160,256]{2,1,0:T(8,128)(2,1)}), bf16[4,160,256]{2,1,0:T(8,128)(2,1)S(1)}, u32[]{:S(2)}, u32[]{:S(2)}) async-start(bf16[4,160,256]{2,1,0:T(8,128)(2,1)} %reduce-scatter.3.cloned.1.call-done), calls=%async_computation.3 | async-start | bytes 655360 | tf_op jit(solution)/shard_map/all_to_all | solution.py:137
  148.6 1.0 fusion.21
  150.8 3.3 %all-to-all-done.2 = bf16[4,160,256]{2,1,0:T(8,128)(2,1)S(1)} async-done(((bf16[4,160,256]{2,1,0:T(8,128)(2,1)}), bf16[4,160,256]{2,1,0:T(8,128)(2,1)S(1)}, u32[]{:S(2)}, u32[]{:S(2)}) %all-to-all-start.2) | async-done | bytes 327712 | tf_op jit(solution)/shard_map/all_to_all | solution.py:137
  154.1 1.0 fusion.17
  155.1 7.4 %convert_bitcast_fusion.1 = bf16[1,2048,896]{2,1,0:T(8,128)(2,1)} fusion(bf16[640,2048]{1,0:T(8,128)(2,1)} %bitcast.115, bf16[640,896]{1,0:T(8,128)(2,1)} %copy-done.18), kind=kOutput, calls=%fused_computation.16 | convolution fusion | flops 2350645248 | bytes 7438336 | tf_op jit(solution)/shard_map/dot_general | solution.py:79
  162.6 4.9 %convert_bitcast_fusion.2 = bf16[1,2048,896]{2,1,0:T(8,128)(2,1)} fusion(bf16[640,2048]{1,0:T(8,128)(2,1)S(1)} %bitcast.117, bf16[640,896]{1,0:T(8,128)(2,1)S(1)} %copy-done.15), kind=kOutput, calls=%fused_computation.17 | convolution fusion | flops 2350645248 | bytes 7438336 | tf_op jit(solution)/shard_map/dot_general | solution.py:76
  167.5 4.6 %convert_bitcast_fusion = bf16[1,896,2048]{2,1,0:T(8,128)(2,1)} fusion(bf16[640,2048]{1,0:T(8,128)(2,1)S(1)} %bitcast.119, f32[640,896]{1,0:T(8,128)S(1)} %copy-done.17, f32[640,896]{1,0:T(8,128)S(1)} %copy-done.16), kind=kOutput, calls=%fused_computation.15 | convolution fusion | flops 2354085888 | bytes 10878976 | tf_op jit(solution)/shard_map/dot_general | solution.py:82
  172.1 4.3 %all-gather.10.cloned.1.call-done = bf16[256,2048]{1,0:T(8,128)(2,1)} async-done(((bf16[256,256]{1,0:T(8,128)(2,1)}), bf16[256,2048]{1,0:T(8,128)(2,1)}) %all-gather.10.cloned.1.call-update) | async-done | bytes 1048592 | tf_op jit(solution)/shard_map/all_gather | solution.py:144
  176.4 1.7 fusion.40
  180.3 7.2 %all-gather = f32[512,1]{0,1:T(1,128)S(1)} all-gather(f32[128,1]{0,1:T(1,128)S(1)} %get-tuple-element.156), channel_id=2, replica_groups=mesh['sp'=4,'tp'=8] {'sp'}, dimensions={0}, use_global_device_ids=true | all-gather | bytes 2560 | tf_op jit(solution)/shard_map/all_gather | solution.py:13
  187.5 7.9 %all-gather.1 = f32[512,1]{0,1:T(1,128)S(1)} all-gather(f32[128,1]{0,1:T(1,128)S(1)} %get-tuple-element.155), channel_id=3, replica_groups=mesh['sp'=4,'tp'=8] {'sp'}, dimensions={0}, use_global_device_ids=true | all-gather | bytes 2560 | tf_op jit(solution)/shard_map/all_gather | solution.py:13
  195.4 1.4 convolution_convert_fusion
  197.5 0.9 fusion.62
  198.6 0.9 fusion.59
  201.1 19.8 %reduce-scatter.5.cloned.1.call-done = bf16[512,128]{1,0:T(8,128)(2,1)} async-done(((bf16[2048,128]{1,0:T(8,128)(2,1)}), bf16[512,128]{1,0:T(8,128)(2,1)}) %reduce-scatter.5.cloned.1.call-update) | async-done | bytes 131088 | tf_op jit(solution)/shard_map/reduce_scatter | solution.py:216
  220.9 0.9 convert_bitcast_fusion.3
  221.8 0.8 copy.95
  (217 shorter events, 8.2 us)
Async XLA Ops:
  7.2 169.2 %copy-start = (bf16[128,2048]{1,0:T(8,128)(2,1)S(1)}, bf16[128,2048]{1,0:T(8,128)(2,1)}, u32[]{:S(2)}) copy-start(bf16[128,2048]{1,0:T(8,128)(2,1)} %param.24) | copy-start | bytes 1572868
  7.2 17.1 %copy-start.2 = (bf16[256,256]{1,0:T(8,128)(2,1)S(1)}, bf16[256,256]{1,0:T(8,128)(2,1)}, u32[]{:S(2)}) copy-start(bf16[256,256]{1,0:T(8,128)(2,1)} %param.17) | copy-start | bytes 393220
  7.2 17.1 %copy-start.13 = (f32[256,2]{0,1:T(2,128)S(1)}, f32[256,2]{0,1:T(2,128)}, u32[]{:S(2)}) copy-start(f32[256,2]{0,1:T(2,128)} %param.20) | copy-start | bytes 6148
  7.2 51.6 %all-gather.6.cloned.1.call-start = ((), (), s32[]{:S(2)}) async-start(), calls=%async_computation.5 | async-start | bytes 2949120 | tf_op jit(solution)/shard_map/all_gather | solution.py:121
  24.2 69.4 %all-gather.8.cloned.1.call-start = ((), (), s32[]{:S(2)}) async-start(), calls=%async_computation.6 | async-start | bytes 2949120 | tf_op jit(solution)/shard_map/all_gather | solution.py:122
  34.1 110.8 %reduce-scatter.3.cloned.1.call-start = ((), (), s32[]{:S(2)}) async-start(), calls=%async_computation.7 | async-start | bytes 2949120 | tf_op jit(solution)/shard_map/reduce_scatter | solution.py:131
  58.8 7.2 %copy-start.8 = (bf16[1,2048,896]{2,1,0:T(8,128)(2,1)S(1)}, bf16[1,2048,896]{2,1,0:T(8,128)(2,1)}, u32[]{:S(2)}) copy-start(bf16[1,2048,896]{2,1,0:T(8,128)(2,1)} %param.22) | copy-start | bytes 11010052
  58.8 7.2 %copy-start.10 = (bf16[4,160,2048]{2,1,0:T(8,128)(2,1)S(1)}, bf16[4,160,2048]{2,1,0:T(8,128)(2,1)}, u32[]{:S(2)}) copy-start(bf16[4,160,2048]{2,1,0:T(8,128)(2,1)} %all-gather.6.cloned.1.call-done) | copy-start | bytes 7864324
  93.6 7.8 %copy-start.7 = (bf16[1,2048,896]{2,1,0:T(8,128)(2,1)S(1)}, bf16[1,2048,896]{2,1,0:T(8,128)(2,1)}, u32[]{:S(2)}) copy-start(bf16[1,2048,896]{2,1,0:T(8,128)(2,1)} %param.21) | copy-start | bytes 11010052
  101.4 3.0 %copy-start.14 = (bf16[640,896]{1,0:T(8,128)(2,1)}, bf16[640,896]{1,0:T(8,128)(2,1)S(1)}, u32[]{:S(2)}) copy-start(bf16[640,896]{1,0:T(8,128)(2,1)S(1)} %get-tuple-element.152) | copy-start | bytes 3440644
  101.4 3.0 %copy-start.18 = (bf16[640,896]{1,0:T(8,128)(2,1)}, bf16[640,896]{1,0:T(8,128)(2,1)S(1)}, u32[]{:S(2)}) copy-start(bf16[640,896]{1,0:T(8,128)(2,1)S(1)} %get-tuple-element.151) | copy-start | bytes 3440644
  101.4 2.9 %copy-start.9 = (bf16[1,2048,896]{2,1,0:T(8,128)(2,1)S(1)}, bf16[1,2048,896]{2,1,0:T(8,128)(2,1)}, u32[]{:S(2)}) copy-start(bf16[1,2048,896]{2,1,0:T(8,128)(2,1)} %param.22) | copy-start | bytes 11010052
  108.6 0.8 copy-start.4
  108.6 41.1 %copy-start.5 = (bf16[128,256]{1,0:T(8,128)(2,1)S(1)}, bf16[128,256]{1,0:T(8,128)(2,1)}, u32[]{:S(2)}) copy-start(bf16[128,256]{1,0:T(8,128)(2,1)} %param.27) | copy-start | bytes 196612
  108.6 41.2 %copy-start.6 = (bf16[128,256]{1,0:T(8,128)(2,1)S(1)}, bf16[128,256]{1,0:T(8,128)(2,1)}, u32[]{:S(2)}) copy-start(bf16[128,256]{1,0:T(8,128)(2,1)} %param.26) | copy-start | bytes 196612
  108.6 41.3 %copy-start.3 = (f32[128,256]{1,0:T(8,128)S(1)}, f32[128,256]{1,0:T(8,128)}, u32[]{:S(2)}) copy-start(f32[128,256]{1,0:T(8,128)} %param.31) | copy-start | bytes 393220
  144.9 9.2 %all-to-all-start.2 = ((bf16[4,160,256]{2,1,0:T(8,128)(2,1)}), bf16[4,160,256]{2,1,0:T(8,128)(2,1)S(1)}, u32[]{:S(2)}, u32[]{:S(2)}) async-start(bf16[4,160,256]{2,1,0:T(8,128)(2,1)} %reduce-scatter.3.cloned.1.call-done), calls=%async_computation.3 | async-start | bytes 655360 | tf_op jit(solution)/shard_map/all_to_all | solution.py:137
  148.5 27.9 %all-gather.10.cloned.1.call-start = ((), (), s32[]{:S(2)}) async-start(), calls=%async_computation.8 | async-start | bytes 1179648 | tf_op jit(solution)/shard_map/all_gather | solution.py:144
  155.1 7.5 %copy-start.15 = (bf16[640,896]{1,0:T(8,128)(2,1)S(1)}, bf16[640,896]{1,0:T(8,128)(2,1)}, u32[]{:S(2)}) copy-start(bf16[640,896]{1,0:T(8,128)(2,1)} %copy-done.14) | copy-start | bytes 3440644
  155.1 65.8 %reduce-scatter.5.cloned.1.call-start = ((), (), s32[]{:S(2)}) async-start(), calls=%async_computation.9 | async-start | bytes 655360 | tf_op jit(solution)/shard_map/reduce_scatter | solution.py:216
  155.1 7.4 %copy-start.11 = (bf16[4,160,2048]{2,1,0:T(8,128)(2,1)S(1)}, bf16[4,160,2048]{2,1,0:T(8,128)(2,1)}, u32[]{:S(2)}) copy-start(bf16[4,160,2048]{2,1,0:T(8,128)(2,1)} %all-gather.6.cloned.1.call-done) | copy-start | bytes 7864324
  162.5 4.9 %copy-start.12 = (bf16[4,160,2048]{2,1,0:T(8,128)(2,1)S(1)}, bf16[4,160,2048]{2,1,0:T(8,128)(2,1)}, u32[]{:S(2)}) copy-start(bf16[4,160,2048]{2,1,0:T(8,128)(2,1)} %all-gather.8.cloned.1.call-done) | copy-start | bytes 7864324
  162.5 4.9 %copy-start.16 = (f32[640,896]{1,0:T(8,128)S(1)}, f32[640,896]{1,0:T(8,128)}, u32[]{:S(2)}) copy-start(f32[640,896]{1,0:T(8,128)} %fusion.3) | copy-start | bytes 6881284
  162.6 4.9 %copy-start.17 = (f32[640,896]{1,0:T(8,128)S(1)}, f32[640,896]{1,0:T(8,128)}, u32[]{:S(2)}) copy-start(f32[640,896]{1,0:T(8,128)} %fusion.7) | copy-start | bytes 6881284
  178.5 16.9 %copy-start.1 = (bf16[256,2048]{1,0:T(8,128)(2,1)S(1)}, bf16[256,2048]{1,0:T(8,128)(2,1)}, u32[]{:S(2)}) copy-start(bf16[256,2048]{1,0:T(8,128)(2,1)} %all-gather.10.cloned.1.call-done) | copy-start | bytes 3145732
Sparse Core Ops, SparseCore 0:
  24.3 34.4 all-gather.5
  60.4 33.1 all-gather.7
  108.7 36.0 reduce-scatter.2
  155.2 21.1 all-gather.9
  196.9 23.9 reduce-scatter.4
where the time goes:
time: 230 us; the launch traced here: 229 us
  waiting for transfers between devices  110 us (48%)
  matrix products  52.8 us (23%)
  blocking collectives  36 us (16%)
  between operations  14.9 us (6%)
  local copies, waits for them, and re-layouts  7.07 us (3%)
  other arithmetic  4.91 us (2%)
  starting transfers between devices  3.85 us (2%)
    reduce_scatter x1, waiting for transfers between devices, local(): lax.psum_scatter(width_part.reshape(experts, capacity, full_width).astype...  34.2 us
    all_gather x1, waiting for transfers between devices, local(): lax.all_gather(part_rows, 'tp', axis=2, tiled=True)  24.6 us
    all_gather x1, waiting for transfers between devices, local(): lax.all_gather(portion_adjoint, 'tp', axis=2, tiled=True)  23.2 us
    reduce_scatter x1, waiting for transfers between devices, local(): lax.psum_scatter(lax.dot_general(full_grad, mixed, (((0,), (1,)), ((), ()...  19.8 us
    all_gather x2, blocking collectives, prefix(): pieces = jax.tree.map(lambda part: lax.all_gather(part, axis), value)  15 us
    all_to_all x1, blocking collectives, local(): lax.all_to_all(sent_rows.reshape(experts, capacity, -1), 'sp', split_axis...  11.7 us
    all_to_all x1, blocking collectives, local(): lax.all_to_all(sent_cot.reshape(experts, capacity, -1), 'sp', split_axis=...  9.32 us
    dot_general x1, matrix products, expert_work(): lax.dot_general(slot_cot, w_down, minor, preferred_element_type=jnp.float32)  7.79 us
  transfers between devices with their start and end apart: 6, of which 6 were waited for; matrix products, arithmetic and copies ran while one was open for 16% of the time, Pallas kernels for 0%

commit v1 on v0

--- a/solution.py
+++ b/solution.py
@@ -1,3 +1,4 @@
+import functools
 import jax
 import jax.numpy as jnp
 from jax import lax
@@ -6,6 +7,21 @@
 HEAD_DIM = 64
 TOP_K = 2
 RATE_SCALE = 8.0
+
+
+def meet_joints(vector, ax_name):
+    return jnp.concatenate(
+        jax.lax.all_to_all(
+            jnp.stack([vector for _ in range(jax.lax.psum(1, axis_name=ax_name))], axis=0),
+            axis_name=ax_name,
+            split_axis=0,
+            concat_axis=0,
+        ),
+        axis=2,
+    )
+
+
+map_tails_here = functools.partial(meet_joints, ax_name="tp")
 
 
 def prefix(value, axis, join, neutral):
@@ -119,7 +135,7 @@
     )
     got_rows, got_cot = (
         lax.all_gather(part_rows, "tp", axis=2, tiled=True),
-        lax.all_gather(portion_adjoint, "tp", axis=2, tiled=True),
+        map_tails_here(portion_adjoint),
     )
     full_width = got_rows.shape[2]
     slot_rows = got_rows.reshape(-1, full_width)

time: 230 us -> 250 us (1.087)
  waiting for transfers between devices: 110 us -> 123 us
  local copies, waits for them, and re-layouts: 7.07 us -> 13.8 us
  starting transfers between devices: 3.85 us -> 8.63 us
  matrix products: 52.8 us -> 48.7 us
    all_to_all x0 -> x1, waiting for transfers between devices: none -> 26.6 us  [meet_joints(): jax.lax.all_to_all(jnp.stack([vector for _ in range(jax.lax.psum(1, axis_...]
    all_gather x1 -> x0, waiting for transfers between devices: 23.2 us -> none  [local(): lax.all_gather(portion_adjoint, 'tp', axis=2, tiled=True)]
    all_gather x1, waiting for transfers between devices: 24.6 us -> 35.1 us  [local(): lax.all_gather(part_rows, 'tp', axis=2, tiled=True)]
    all_to_all x0 -> x1, starting transfers between devices: none -> 4.87 us  [meet_joints(): jax.lax.all_to_all(jnp.stack([vector for _ in range(jax.lax.psum(1, axis_...]
    dot_general x1, matrix products: 7.79 us -> 3.54 us  [expert_work(): lax.dot_general(slot_cot, w_down, minor, preferred_element_type=jnp.float32)]
    unnamed x46 -> x59, local copies, waits for them, and re-layouts: 4.49 us -> 7.89 us
  transfers between devices with their start and end apart: 6 -> 6, of which waited for: 6 -> 6; matrix products, arithmetic and copies ran while one was open for 16% -> 15% of each run, Pallas kernels for 0% -> 0%
where the time goes in v1:
time: 250 us; the launch traced here: 249 us
  waiting for transfers between devices  123 us (49%)
  matrix products  48.7 us (19%)
  blocking collectives  35.4 us (14%)
  between operations  14.9 us (6%)
  local copies, waits for them, and re-layouts  13.8 us (6%)
  starting transfers between devices  8.63 us (3%)
  other arithmetic  4.89 us (2%)
    all_gather x1, waiting for transfers between devices, local(): lax.all_gather(part_rows, 'tp', axis=2, tiled=True)  35.1 us
    reduce_scatter x1, waiting for transfers between devices, local(): lax.psum_scatter(width_part.reshape(experts, capacity, full_width).astype...  34 us
    all_to_all x1, waiting for transfers between devices, meet_joints(): jax.lax.all_to_all(jnp.stack([vector for _ in range(jax.lax.psum(1, axis_...  26.6 us
    reduce_scatter x1, waiting for transfers between devices, local(): lax.psum_scatter(lax.dot_general(full_grad, mixed, (((0,), (1,)), ((), ()...  19.8 us
    all_gather x2, blocking collectives, prefix(): pieces = jax.tree.map(lambda part: lax.all_gather(part, axis), value)  15 us
    all_to_all x1, blocking collectives, local(): lax.all_to_all(sent_rows.reshape(experts, capacity, -1), 'sp', split_axis...  11.7 us
    all_to_all x1, blocking collectives, local(): lax.all_to_all(sent_cot.reshape(experts, capacity, -1), 'sp', split_axis=...  8.62 us
    unnamed x59, local copies, waits for them, and re-layouts  7.89 us
  transfers between devices with their start and end apart: 6, of which 6 were waited for; matrix products, arithmetic and copies ran while one was open for 15% of the time, Pallas kernels for 0%

profile of v1, /device:TPU:0, one launch (start us, length us, event | category | flops | bytes accessed | tf_op | source)
XLA Modules:
  0.0 249.5 jit_solution(7711154814992926171)
XLA Ops:
  8.4 1.2 reduce-window.6
  12.2 1.1 convolution_convert_fusion.1
  13.4 11.7 %all_to_all.20 = bf16[4,160,256]{2,1,0:T(8,128)(2,1)} all-to-all(bf16[4,160,256]{2,1,0:T(8,128)(2,1)S(1)} %bitcast.108), channel_id=1, replica_groups=mesh['sp'=4,'tp'=8] {'sp'}, dimensions={0} | all-to-all | bytes 655360 | tf_op jit(solution)/shard_map/all_to_all | solution.py:129
  25.6 8.6 %all_to_all.21 = bf16[4,160,256]{2,1,0:T(8,128)(2,1)S(1)} all-to-all(bf16[4,160,256]{2,1,0:T(8,128)(2,1)S(1)} %bitcast.111), channel_id=1, replica_groups=mesh['sp'=4,'tp'=8] {'sp'}, dimensions={0} | all-to-all | bytes 655360 | tf_op jit(solution)/shard_map/all_to_all | solution.py:132
  34.2 1.8 stack.2
  36.0 4.9 %all-to-all-start.2 = ((bf16[8,4,160,256]{3,2,1,0:T(8,128)(2,1)}), bf16[8,4,160,256]{3,2,1,0:T(8,128)(2,1)S(1)}, u32[]{:S(2)}, u32[]{:S(2)}) async-start(bf16[8,4,160,256]{3,2,1,0:T(8,128)(2,1)} %stack.2), calls=%async_computation.2 | async-start | bytes 5242880 | tf_op jit(solution)/shard_map/all_to_all | solution.py:14
  40.9 35.1 %all-gather.5.cloned.1.call-done = bf16[4,160,2048]{2,1,0:T(8,128)(2,1)} async-done(((bf16[4,160,256]{2,1,0:T(8,128)(2,1)}), bf16[4,160,2048]{2,1,0:T(8,128)(2,1)}) %all-gather.5.cloned.1.call-update) | async-done | bytes 2621456 | tf_op jit(solution)/shard_map/all_gather | solution.py:137
  76.0 7.3 %fusion.3 = f32[640,896]{1,0:T(8,128)} fusion(bf16[640,2048]{1,0:T(8,128)(2,1)} %bitcast.121, bf16[1,2048,896]{2,1,0:T(8,128)(2,1)} %param.21), kind=kOutput, calls=%fused_computation.7 | convolution fusion | flops 2348810240 | bytes 8585216 | tf_op jit(solution)/shard_map/dot_general | solution.py:75
  83.3 4.3 %fusion.7 = f32[640,896]{1,0:T(8,128)} fusion(bf16[640,2048]{1,0:T(8,128)(2,1)S(1)} %bitcast.123, bf16[1,2048,896]{2,1,0:T(8,128)(2,1)S(1)} %copy-done.13), kind=kOutput, calls=%fused_computation.11 | convolution fusion | flops 2348810240 | bytes 8585216 | tf_op jit(solution)/shard_map/dot_general | solution.py:76
  87.6 26.6 %all-to-all-done.2 = bf16[8,4,160,256]{3,2,1,0:T(8,128)(2,1)S(1)} async-done(((bf16[8,4,160,256]{3,2,1,0:T(8,128)(2,1)}), bf16[8,4,160,256]{3,2,1,0:T(8,128)(2,1)S(1)}, u32[]{:S(2)}, u32[]{:S(2)}) %all-to-all-start.2) | async-done | bytes 2621472 | tf_op jit(solution)/shard_map/all_to_all | solution.py:14
  114.2 1.5 copy.104
  116.6 1.6 copy-done.11
  118.2 3.5 %multiply_convert_fusion.1 = (bf16[640,896]{1,0:T(8,128)(2,1)S(1)}, bf16[640,896]{1,0:T(8,128)(2,1)S(1)}) fusion(f32[640,896]{1,0:T(8,128)S(1)} %copy-done.20, f32[640,896]{1,0:T(8,128)S(1)} %copy-done.22, bf16[640,2048]{1,0:T(8,128)(2,1)S(1)} %bitcast.104, bf16[1,896,2048]{2,1,0:T(8,128)(2,1)S(1)} %copy-done.11), kind=kOutput, calls=%fused_computation.20 | convolution fusion | flops 2356264960 | bytes 13172736 | tf_op jit(solution)/shard_map/dot_general | solution.py:80
  121.8 2.9 %fusion.1 = f32[640,2048]{1,0:T(8,128)S(1)} fusion(bf16[640,896]{1,0:T(8,128)(2,1)S(1)} %get-tuple-element.158, bf16[1,2048,896]{2,1,0:T(8,128)(2,1)S(1)} %copy-done.12), kind=kOutput, calls=%fused_computation.5 | convolution fusion | flops 2348810240 | bytes 10059776 | tf_op jit(solution)/shard_map/dot_general | solution.py:85
  124.8 4.4 %add_convert_fusion = bf16[640,2048]{1,0:T(8,128)(2,1)} fusion(f32[640,2048]{1,0:T(8,128)S(1)} %fusion.1, bf16[640,896]{1,0:T(8,128)(2,1)S(1)} %get-tuple-element.157, bf16[1,2048,896]{2,1,0:T(8,128)(2,1)S(1)} %copy-done.14), kind=kOutput, calls=%fused_computation.4 | convolution fusion | flops 2351431680 | bytes 12681216 | tf_op jit(solution)/shard_map/dot_general | solution.py:86
  130.1 1.0 fusion.23
  131.2 34.0 %reduce-scatter.3.cloned.1.call-done = bf16[4,160,256]{2,1,0:T(8,128)(2,1)} async-done(((bf16[4,160,2048]{2,1,0:T(8,128)(2,1)}), bf16[4,160,256]{2,1,0:T(8,128)(2,1)}) %reduce-scatter.3.cloned.1.call-update) | async-done | bytes 327696 | tf_op jit(solution)/shard_map/reduce_scatter | solution.py:147
  165.2 3.6 %all-to-all-start.3 = ((bf16[4,160,256]{2,1,0:T(8,128)(2,1)}), bf16[4,160,256]{2,1,0:T(8,128)(2,1)S(1)}, u32[]{:S(2)}, u32[]{:S(2)}) async-start(bf16[4,160,256]{2,1,0:T(8,128)(2,1)} %reduce-scatter.3.cloned.1.call-done), calls=%async_computation.4 | async-start | bytes 655360 | tf_op jit(solution)/shard_map/all_to_all | solution.py:153
  168.8 1.0 fusion.21
  171.1 3.3 %all-to-all-done.3 = bf16[4,160,256]{2,1,0:T(8,128)(2,1)S(1)} async-done(((bf16[4,160,256]{2,1,0:T(8,128)(2,1)}), bf16[4,160,256]{2,1,0:T(8,128)(2,1)S(1)}, u32[]{:S(2)}, u32[]{:S(2)}) %all-to-all-start.3) | async-done | bytes 327712 | tf_op jit(solution)/shard_map/all_to_all | solution.py:153
  174.4 1.0 fusion.17
  175.5 7.4 %convert_bitcast_fusion.1 = bf16[1,2048,896]{2,1,0:T(8,128)(2,1)} fusion(bf16[640,2048]{1,0:T(8,128)(2,1)} %bitcast.122, bf16[640,896]{1,0:T(8,128)(2,1)} %copy-done.24), kind=kOutput, calls=%fused_computation.16 | convolution fusion | flops 2350645248 | bytes 7438336 | tf_op jit(solution)/shard_map/dot_general | solution.py:95
  182.9 4.9 %convert_bitcast_fusion.2 = bf16[1,2048,896]{2,1,0:T(8,128)(2,1)} fusion(bf16[640,2048]{1,0:T(8,128)(2,1)S(1)} %bitcast.124, bf16[640,896]{1,0:T(8,128)(2,1)S(1)} %copy-done.19), kind=kOutput, calls=%fused_computation.17 | convolution fusion | flops 2350645248 | bytes 7438336 | tf_op jit(solution)/shard_map/dot_general | solution.py:92
  187.8 4.6 %convert_bitcast_fusion = bf16[1,896,2048]{2,1,0:T(8,128)(2,1)} fusion(bf16[640,2048]{1,0:T(8,128)(2,1)S(1)} %bitcast.105, f32[640,896]{1,0:T(8,128)S(1)} %copy-done.23, f32[640,896]{1,0:T(8,128)S(1)} %copy-done.21), kind=kOutput, calls=%fused_computation.15 | convolution fusion | flops 2354085888 | bytes 10878976 | tf_op jit(solution)/shard_map/dot_general | solution.py:98
  192.4 4.3 %all-gather.7.cloned.1.call-done = bf16[256,2048]{1,0:T(8,128)(2,1)} async-done(((bf16[256,256]{1,0:T(8,128)(2,1)}), bf16[256,2048]{1,0:T(8,128)(2,1)}) %all-gather.7.cloned.1.call-update) | async-done | bytes 1048592 | tf_op jit(solution)/shard_map/all_gather | solution.py:160
  196.7 1.8 fusion.40
  200.6 7.2 %all-gather = f32[512,1]{0,1:T(1,128)S(1)} all-gather(f32[128,1]{0,1:T(1,128)S(1)} %get-tuple-element.162), channel_id=2, replica_groups=mesh['sp'=4,'tp'=8] {'sp'}, dimensions={0}, use_global_device_ids=true | all-gather | bytes 2560 | tf_op jit(solution)/shard_map/all_gather | solution.py:29
  207.7 7.9 %all-gather.1 = f32[512,1]{0,1:T(1,128)S(1)} all-gather(f32[128,1]{0,1:T(1,128)S(1)} %get-tuple-element.161), channel_id=3, replica_groups=mesh['sp'=4,'tp'=8] {'sp'}, dimensions={0}, use_global_device_ids=true | all-gather | bytes 2560 | tf_op jit(solution)/shard_map/all_gather | solution.py:29
  215.7 1.4 convolution_convert_fusion
  217.8 0.9 fusion.62
  221.4 19.8 %reduce-scatter.5.cloned.1.call-done = bf16[512,128]{1,0:T(8,128)(2,1)} async-done(((bf16[2048,128]{1,0:T(8,128)(2,1)}), bf16[512,128]{1,0:T(8,128)(2,1)}) %reduce-scatter.5.cloned.1.call-update) | async-done | bytes 131088 | tf_op jit(solution)/shard_map/reduce_scatter | solution.py:232
  241.2 0.9 convert_bitcast_fusion.3
  (231 shorter events, 13.2 us)
Async XLA Ops:
  7.2 189.5 %copy-start = (bf16[128,2048]{1,0:T(8,128)(2,1)S(1)}, bf16[128,2048]{1,0:T(8,128)(2,1)}, u32[]{:S(2)}) copy-start(bf16[128,2048]{1,0:T(8,128)(2,1)} %param.24) | copy-start | bytes 1572868
  7.2 17.9 %copy-start.6 = (bf16[256,256]{1,0:T(8,128)(2,1)S(1)}, bf16[256,256]{1,0:T(8,128)(2,1)}, u32[]{:S(2)}) copy-start(bf16[256,256]{1,0:T(8,128)(2,1)} %param.17) | copy-start | bytes 393220
  7.2 18.0 %copy-start.17 = (f32[256,2]{0,1:T(2,128)S(1)}, f32[256,2]{0,1:T(2,128)}, u32[]{:S(2)}) copy-start(f32[256,2]{0,1:T(2,128)} %param.20) | copy-start | bytes 6148
  7.2 68.8 %all-gather.5.cloned.1.call-start = ((), (), s32[]{:S(2)}) async-start(), calls=%async_computation.6 | async-start | bytes 2949120 | tf_op jit(solution)/shard_map/all_gather | solution.py:137
  11.3 0.9 copy-start.1
  36.0 78.1 %all-to-all-start.2 = ((bf16[8,4,160,256]{3,2,1,0:T(8,128)(2,1)}), bf16[8,4,160,256]{3,2,1,0:T(8,128)(2,1)S(1)}, u32[]{:S(2)}, u32[]{:S(2)}) async-start(bf16[8,4,160,256]{3,2,1,0:T(8,128)(2,1)} %stack.2), calls=%async_computation.2 | async-start | bytes 5242880 | tf_op jit(solution)/shard_map/all_to_all | solution.py:14
  40.9 124.3 %reduce-scatter.3.cloned.1.call-start = ((), (), s32[]{:S(2)}) async-start(), calls=%async_computation.7 | async-start | bytes 2949120 | tf_op jit(solution)/shard_map/reduce_scatter | solution.py:147
  76.0 7.3 %copy-start.13 = (bf16[1,2048,896]{2,1,0:T(8,128)(2,1)S(1)}, bf16[1,2048,896]{2,1,0:T(8,128)(2,1)}, u32[]{:S(2)}) copy-start(bf16[1,2048,896]{2,1,0:T(8,128)(2,1)} %param.22) | copy-start | bytes 11010052
  76.0 7.3 %copy-start.15 = (bf16[4,160,2048]{2,1,0:T(8,128)(2,1)S(1)}, bf16[4,160,2048]{2,1,0:T(8,128)(2,1)}, u32[]{:S(2)}) copy-start(bf16[4,160,2048]{2,1,0:T(8,128)(2,1)} %all-gather.5.cloned.1.call-done) | copy-start | bytes 7864324
  114.1 2.4 copy-start.20
  114.2 2.4 copy-start.22
  115.7 2.6 %copy-start.11 = (bf16[1,896,2048]{2,1,0:T(8,128)(2,1)S(1)}, bf16[1,896,2048]{2,1,0:T(8,128)(2,1)}, u32[]{:S(2)}) copy-start(bf16[1,896,2048]{2,1,0:T(8,128)(2,1)} %param.23) | copy-start | bytes 11010052
  116.6 5.2 %copy-start.3 = (bf16[80,8,8,256]{3,1,2,0:T(8,128)(2,1)}, bf16[80,8,8,256]{3,1,2,0:T(8,128)(2,1)S(1)}, u32[]{:S(2)}) copy-start(bf16[80,8,8,256]{3,1,2,0:T(8,128)(2,1)S(1)} %copy.133) | copy-start | bytes 7864324
  118.2 3.6 %copy-start.12 = (bf16[1,2048,896]{2,1,0:T(8,128)(2,1)S(1)}, bf16[1,2048,896]{2,1,0:T(8,128)(2,1)}, u32[]{:S(2)}) copy-start(bf16[1,2048,896]{2,1,0:T(8,128)(2,1)} %param.21) | copy-start | bytes 11010052
  121.8 3.0 %copy-start.18 = (bf16[640,896]{1,0:T(8,128)(2,1)}, bf16[640,896]{1,0:T(8,128)(2,1)S(1)}, u32[]{:S(2)}) copy-start(bf16[640,896]{1,0:T(8,128)(2,1)S(1)} %get-tuple-element.158) | copy-start | bytes 3440644
  121.8 3.0 %copy-start.24 = (bf16[640,896]{1,0:T(8,128)(2,1)}, bf16[640,896]{1,0:T(8,128)(2,1)S(1)}, u32[]{:S(2)}) copy-start(bf16[640,896]{1,0:T(8,128)(2,1)S(1)} %get-tuple-element.157) | copy-start | bytes 3440644
  121.8 2.9 %copy-start.14 = (bf16[1,2048,896]{2,1,0:T(8,128)(2,1)S(1)}, bf16[1,2048,896]{2,1,0:T(8,128)(2,1)}, u32[]{:S(2)}) copy-start(bf16[1,2048,896]{2,1,0:T(8,128)(2,1)} %param.22) | copy-start | bytes 11010052
  129.1 0.8 copy-start.8
  129.1 40.8 %copy-start.9 = (bf16[128,256]{1,0:T(8,128)(2,1)S(1)}, bf16[128,256]{1,0:T(8,128)(2,1)}, u32[]{:S(2)}) copy-start(bf16[128,256]{1,0:T(8,128)(2,1)} %param.27) | copy-start | bytes 196612
  129.1 40.9 %copy-start.10 = (bf16[128,256]{1,0:T(8,128)(2,1)S(1)}, bf16[128,256]{1,0:T(8,128)(2,1)}, u32[]{:S(2)}) copy-start(bf16[128,256]{1,0:T(8,128)(2,1)} %param.26) | copy-start | bytes 196612
  129.1 41.1 %copy-start.7 = (f32[128,256]{1,0:T(8,128)S(1)}, f32[128,256]{1,0:T(8,128)}, u32[]{:S(2)}) copy-start(f32[128,256]{1,0:T(8,128)} %param.31) | copy-start | bytes 393220
  129.1 45.2 %copy-start.2 = (s32[640,256]{1,0:T(8,128)S(1)}, s32[640,256]{1,0:T(8,128)}, u32[]{:S(2)}) copy-start(s32[640,256]{1,0:T(8,128)} %copy-done.1) | copy-start | bytes 1966084
  165.2 9.2 %all-to-all-start.3 = ((bf16[4,160,256]{2,1,0:T(8,128)(2,1)}), bf16[4,160,256]{2,1,0:T(8,128)(2,1)S(1)}, u32[]{:S(2)}, u32[]{:S(2)}) async-start(bf16[4,160,256]{2,1,0:T(8,128)(2,1)} %reduce-scatter.3.cloned.1.call-done), calls=%async_computation.4 | async-start | bytes 655360 | tf_op jit(solution)/shard_map/all_to_all | solution.py:153
  168.8 27.8 %all-gather.7.cloned.1.call-start = ((), (), s32[]{:S(2)}) async-start(), calls=%async_computation.8 | async-start | bytes 1179648 | tf_op jit(solution)/shard_map/all_gather | solution.py:160
  175.4 7.5 %copy-start.19 = (bf16[640,896]{1,0:T(8,128)(2,1)S(1)}, bf16[640,896]{1,0:T(8,128)(2,1)}, u32[]{:S(2)}) copy-start(bf16[640,896]{1,0:T(8,128)(2,1)} %copy-done.18) | copy-start | bytes 3440644
  175.4 65.8 %reduce-scatter.5.cloned.1.call-start = ((), (), s32[]{:S(2)}) async-start(), calls=%async_computation.9 | async-start | bytes 655360 | tf_op jit(solution)/shard_map/reduce_scatter | solution.py:232
  175.5 7.4 %copy-start.16 = (bf16[4,160,2048]{2,1,0:T(8,128)(2,1)S(1)}, bf16[4,160,2048]{2,1,0:T(8,128)(2,1)}, u32[]{:S(2)}) copy-start(bf16[4,160,2048]{2,1,0:T(8,128)(2,1)} %all-gather.5.cloned.1.call-done) | copy-start | bytes 7864324
  182.9 4.9 %copy-start.4 = (bf16[80,8,8,256]{3,1,2,0:T(8,128)(2,1)S(1)}, bf16[80,8,8,256]{3,1,2,0:T(8,128)(2,1)}, u32[]{:S(2)}) copy-start(bf16[80,8,8,256]{3,1,2,0:T(8,128)(2,1)} %copy-done.3) | copy-start | bytes 7864324
  182.9 4.9 %copy-start.21 = (f32[640,896]{1,0:T(8,128)S(1)}, f32[640,896]{1,0:T(8,128)}, u32[]{:S(2)}) copy-start(f32[640,896]{1,0:T(8,128)} %fusion.3) | copy-start | bytes 6881284
  182.9 4.9 %copy-start.23 = (f32[640,896]{1,0:T(8,128)S(1)}, f32[640,896]{1,0:T(8,128)}, u32[]{:S(2)}) copy-start(f32[640,896]{1,0:T(8,128)} %fusion.7) | copy-start | bytes 6881284
  198.8 16.9 %copy-start.5 = (bf16[256,2048]{1,0:T(8,128)(2,1)S(1)}, bf16[256,2048]{1,0:T(8,128)(2,1)}, u32[]{:S(2)}) copy-start(bf16[256,2048]{1,0:T(8,128)(2,1)} %all-gather.7.cloned.1.call-done) | copy-start | bytes 3145732
Sparse Core Ops, SparseCore 0:
  25.2 50.7 all-gather.4
  129.3 35.8 reduce-scatter.2
  175.5 21.1 all-gather.6
  217.2 23.9 reduce-scatter.4
